TPU v7x, 32 devices: a whole 2x2x4 slice. The times are simulated.
32 devices in a mesh: kv: 8 (over z, x), tp: 4 (over y, core).
Axes of the slice: x: 2, y: 2, z: 4, core: 2. Of those that a mesh axis runs over, the one named last changes fastest.
Arguments:
- tokens: bfloat16 [22, 4096], P(None, ('kv', 'tp')), may hold values from -22 to 22
- attn_gain: float32 [4096], P('kv'), may hold values from 0.1 to 1.9
- w_query: bfloat16 [4096, 4096], P('kv', 'tp'), may hold values from -0.09375 to 0.09375
- w_key: bfloat16 [4096, 4096], P('kv', 'tp'), may hold values from -0.5 to 0.5
- w_value: bfloat16 [4096, 4096], P('kv', 'tp'), may hold values from -0.09375 to 0.09375
- cache_keys: bfloat16 [22, 2048, 32, 128], P(None, 'kv', 'tp'), may hold values from -256 to 256
- cache_values: bfloat16 [22, 2048, 32, 128], P(None, 'kv', 'tp'), may hold values from -6 to 6
- lambdas: float32 [32], P('tp'), may hold values from 0.3 to 0.8
- head_gain: float32 [128], replicated, may hold values from 0.1 to 1.9
- w_out: bfloat16 [4096, 4096], P('tp', 'kv'), may hold values from -0.09375 to 0.09375
- mlp_gain: float32 [4096], P('kv'), may hold values from 0.1 to 1.9
- w_gate: bfloat16 [4096, 11008], P('kv', 'tp'), may hold values from -0.09375 to 0.09375
- w_up: bfloat16 [4096, 11008], P('kv', 'tp'), may hold values from -0.09375 to 0.09375
- w_down: bfloat16 [11008, 4096], P('tp', 'kv'), may hold values from -0.0546875 to 0.0546875
Outputs:
- output: bfloat16 [22, 4096], P(None, ('kv', 'tp'))
All inputs are finite; a program needn't handle non-finite values.
Results may differ from a plain program's by a relative error of at most 0.017.
The roundings to bfloat16 on the way count: a program that leaves them out, or rounds other values in their place, can miss the bound.
Values may be sent and summed in bfloat16 or wider, within the bound.
A program may use at most 128 MiB of HBM per device.

v0:
```python
import jax
import jax.numpy as jnp
from jax import lax
from jax.sharding import PartitionSpec as P

D = 4096
epsilon = 1e-06


def combined_all(value, axis, join):
    pieces = jax.tree.map(lambda part: lax.all_gather(part, axis), value)
    head = jax.tree.map(lambda part: part[0], pieces)
    tail = jax.tree.map(lambda part: part[1:], pieces)
    running, _ = lax.scan(lambda running, section: (join(running, section), None), head, tail)
    return running


def join_map(left_max, left_sum, left_val, right_max, right_sum, right_val):
    peak_val = jnp.maximum(left_max, right_max)
    left_weight = jnp.exp(left_max - peak_val)
    right_weight = jnp.exp(right_max - peak_val)
    return (
        peak_val,
        left_sum * left_weight + right_sum * right_weight,
        left_val * left_weight[..., None] + right_val * right_weight[..., None],
    )


def combine(earlier, later):
    return join_map(earlier[0], earlier[1], earlier[2], later[0], later[1], later[2]) + join_map(
        earlier[3], earlier[4], earlier[5], later[3], later[4], later[5]
    )


def per_device(
    tokens,
    attn_gain,
    w_query,
    w_key,
    w_value,
    cache_keys,
    cache_values,
    lambdas,
    head_gain,
    w_out,
    mlp_gain,
    w_gate,
    w_up,
    w_down,
):
    seq_count = tokens.shape[0]
    own_width = tokens.shape[1]
    local_heads = lambdas.shape[0]
    head_dim = head_gain.shape[0]
    half_dim = head_dim // 2
    score_scale = half_dim ** (-0.5)
    gathered = lax.all_gather(tokens, "tp", axis=1, tiled=True)
    gathered_f = gathered.astype(jnp.float32)
    normed_in = (gathered_f * attn_gain).astype(jnp.bfloat16)
    query_part = jnp.dot(normed_in, w_query, preferred_element_type=jnp.float32)
    key_part = jnp.dot(normed_in, w_key, preferred_element_type=jnp.float32)
    value_part = jnp.dot(normed_in, w_value, preferred_element_type=jnp.float32)
    query_sum, key_sum, value_sum, square_sum = lax.psum(
        (query_part, key_part, value_part, jnp.sum(gathered_f * gathered_f, axis=1, keepdims=True)),
        "kv",
    )
    scale_in = lax.rsqrt(square_sum / D + epsilon)
    query_rows = (
        (scale_in * query_sum).astype(jnp.bfloat16).reshape(seq_count, local_heads, head_dim)
    )
    key_new = (scale_in * key_sum).astype(jnp.bfloat16).reshape(seq_count, local_heads, head_dim)
    value_new = (
        (scale_in * value_sum).astype(jnp.bfloat16).reshape(seq_count, local_heads, head_dim)
    )

    def partial_map(low, high):
        scores = (
            jnp.einsum(
                "shd,sthd->sht",
                query_rows[:, :, low:high],
                cache_keys[:, :, :, low:high],
                preferred_element_type=jnp.float32,
            )
            * score_scale
        )
        maxima = jnp.max(scores, axis=2)
        weights = jnp.exp(scores - maxima[:, :, None])
        totals = jnp.sum(weights, axis=2)
        summed = jnp.einsum(
            "sht,sthd->shd",
            weights.astype(jnp.bfloat16),
            cache_values,
            preferred_element_type=jnp.float32,
        )
        return (maxima, totals, summed)

    def own_term(low, high):
        score_new = (
            jnp.sum(
                query_rows[:, :, low:high].astype(jnp.float32)
                * key_new[:, :, low:high].astype(jnp.float32),
                axis=2,
            )
            * score_scale
        )
        return (score_new, jnp.ones_like(score_new), value_new.astype(jnp.float32))

    first_part = partial_map(0, half_dim)
    second_part = partial_map(half_dim, head_dim)
    merged = combined_all(
        (
            first_part[0],
            first_part[1],
            first_part[2],
            second_part[0],
            second_part[1],
            second_part[2],
        ),
        "kv",
        combine,
    )
    combined = combine(merged, own_term(0, half_dim) + own_term(half_dim, head_dim))
    first_map = combined[2] / combined[1][:, :, None]
    second_map = combined[5] / combined[4][:, :, None]
    difference = first_map - lambdas[None, :, None] * second_map
    normed = (
        difference
        * lax.rsqrt(jnp.mean(difference * difference, axis=2, keepdims=True) + epsilon)
        * head_gain
    )
    heads_out = normed.astype(jnp.bfloat16).reshape(seq_count, local_heads * head_dim)
    branch = lax.psum(
        jnp.dot(heads_out, w_out, preferred_element_type=jnp.float32).astype(jnp.bfloat16), "tp"
    ).astype(jnp.float32)
    residual = (gathered_f + branch).astype(jnp.bfloat16)
    residual_f = residual.astype(jnp.float32)
    mid_sum = lax.psum(jnp.sum(residual_f * residual_f, axis=1, keepdims=True), "kv")
    scale_mid = lax.rsqrt(mid_sum / D + epsilon)
    normed_mid = (residual_f * mlp_gain).astype(jnp.bfloat16)
    gate_part = jnp.dot(normed_mid, w_gate, preferred_element_type=jnp.float32)
    up_part = jnp.dot(normed_mid, w_up, preferred_element_type=jnp.float32)
    gate_sum, up_sum = lax.psum((gate_part, up_part), "kv")
    hidden = (jax.nn.silu(scale_mid * gate_sum) * (scale_mid * up_sum)).astype(jnp.bfloat16)
    down_part = jnp.dot(hidden, w_down, preferred_element_type=jnp.float32).astype(jnp.bfloat16)
    mixer_own = lax.psum_scatter(down_part, "tp", scatter_dimension=1, tiled=True).astype(
        jnp.float32
    )
    tp_index = lax.axis_index("tp")
    residual_own = lax.dynamic_slice_in_dim(residual_f, tp_index * own_width, own_width, 1)
    return (residual_own + mixer_own).astype(jnp.bfloat16)


def solution(mesh):
    in_specs = (
        P(None, ("kv", "tp")),
        P("kv"),
        P("kv", "tp"),
        P("kv", "tp"),
        P("kv", "tp"),
        P(None, "kv", "tp", None),
        P(None, "kv", "tp", None),
        P("tp"),
        P(),
        P("tp", "kv"),
        P("kv"),
        P("kv", "tp"),
        P("kv", "tp"),
        P("tp", "kv"),
    )
    out_specs = P(None, ("kv", "tp"))
    return jax.shard_map(
        per_device, mesh=mesh, in_specs=in_specs, out_specs=out_specs, check_vma=False
    )
```

profile of v0, /device:TPU:0, one launch (start us, length us, event | category | flops | bytes accessed | tf_op | source)
XLA Modules:
  0.0 441.2 jit_solution(7946327300778123110)
XLA Ops:
  6.5 6.5 %all_gather.39 = bf16[22,512]{1,0:T(8,128)(2,1)S(1)} all-gather(bf16[22,128]{1,0:T(8,128)(2,1)} %param.16), channel_id=1, replica_groups=mesh['kv'=8,'tp'=4] {'tp'}, dimensions={1}, use_global_device_ids=true | all-gather | bytes 28160 | tf_op jit(solution)/shard_map/all_gather | solution.py:57
  13.0 2.1 fusion.35
  15.2 2.1 fusion.33
  17.3 2.1 fusion.37
  19.5 17.3 %fusion.54 = (bf16[22,256,8,64]{3,2,1,0:T(8,128)(2,1)}, bf16[22,256,8,64]{3,2,1,0:T(8,128)(2,1)}) fusion(bf16[22,256,8,128]{3,2,1,0:T(8,128)(2,1)} %param.21), kind=kLoop, calls=%fused_computation.89 | loop fusion | bytes 23068672 | tf_op jit(solution)/shard_map/slice | solution.py:81
  36.9 22.2 %psum.56 = f32[22,1]{0,1:T(1,128)S(1)} all-reduce(f32[22,1]{0,1:T(1,128)S(1)} %bitcast.129), channel_id=1, replica_groups=mesh['kv'=8,'tp'=4] {'kv'}, use_global_device_ids=true, to_apply=%region_1.0 | all-reduce | flops 22 | bytes 176 | tf_op jit(solution)/shard_map/psum | solution.py:63
  59.1 34.2 %all-reduce.7.cloned.1.call-done = (f32[22,1024]{1,0:T(8,128)}, f32[22,1024]{1,0:T(8,128)}, f32[22,1024]{1,0:T(8,128)}) async-done(((f32[22,1024]{1,0:T(8,128)}, f32[22,1024]{1,0:T(8,128)}, f32[22,1024]{1,0:T(8,128)}), (f32[22,1024]{1,0:T(8,128)}, f32[22,1024]{1,0:T(8,128)}, f32[22,1024]{1,0:T(8,128)})) %all-reduce.7.cloned.1.call-update) | async-done | bytes 270352 | tf_op jit(solution)/shard_map/psum | solution.py:63
  94.5 7.4 %fusion.6 = f32[22,8,1,256]{3,2,1,0:T(1,128)S(1)} fusion(bf16[22,256,8,64]{3,2,1,0:T(8,128)(2,1)} %get-tuple-element.134, bf16[22,8,64,1]{2,1,0,3:T(8,128)(2,1)S(1)} %get-tuple-element.142), kind=kOutput, calls=%fused_computation.16 | convolution fusion | flops 5767168 | bytes 5969920 | tf_op jit(solution)/shard_map/shd,sthd->sht/dot_general | solution.py:78
  102.2 30.6 %all-gather.8 = f32[8,22,8]{1,2,0:T(8,128)S(1)} all-gather(f32[1,22,8]{1,2,0:T(8,128)S(1)} %copy.59), channel_id=5, replica_groups=mesh['kv'=8,'tp'=4] {'kv'}, dimensions={0}, use_global_device_ids=true | all-gather | bytes 6336 | tf_op jit(solution)/shard_map/all_gather | solution.py:11
  132.9 30.6 %all-gather.9 = f32[8,22,8]{1,2,0:T(8,128)S(1)} all-gather(f32[1,22,8]{1,2,0:T(8,128)S(1)} %copy.60), channel_id=6, replica_groups=mesh['kv'=8,'tp'=4] {'kv'}, dimensions={0}, use_global_device_ids=true | all-gather | bytes 6336 | tf_op jit(solution)/shard_map/all_gather | solution.py:11
  163.5 7.4 %fusion.8 = f32[22,8,1,256]{3,2,1,0:T(1,128)S(1)} fusion(bf16[22,256,8,64]{3,2,1,0:T(8,128)(2,1)} %get-tuple-element.135, bf16[22,8,64,1]{2,1,0,3:T(8,128)(2,1)S(1)} %get-tuple-element.143), kind=kOutput, calls=%fused_computation.18 | convolution fusion | flops 5767168 | bytes 5969920 | tf_op jit(solution)/shard_map/shd,sthd->sht/dot_general | solution.py:78
  171.2 30.6 %all-gather.6 = f32[8,22,8]{1,2,0:T(8,128)S(1)} all-gather(f32[1,22,8]{1,2,0:T(8,128)S(1)} %copy.57), channel_id=2, replica_groups=mesh['kv'=8,'tp'=4] {'kv'}, dimensions={0}, use_global_device_ids=true | all-gather | bytes 6336 | tf_op jit(solution)/shard_map/all_gather | solution.py:11
  201.9 30.6 %all-gather.7 = f32[8,22,8]{1,2,0:T(8,128)S(1)} all-gather(f32[1,22,8]{1,2,0:T(8,128)S(1)} %copy.58), channel_id=3, replica_groups=mesh['kv'=8,'tp'=4] {'kv'}, dimensions={0}, use_global_device_ids=true | all-gather | bytes 6336 | tf_op jit(solution)/shard_map/all_gather | solution.py:11
  232.5 5.9 %fusion.12 = f32[22,8,1,128]{3,2,1,0:T(1,128)S(1)} fusion(bf16[22,256,8,128]{3,2,1,0:T(8,128)(2,1)} %param.22, bf16[22,8,256,1]{2,1,0,3:T(8,128)(2,1)S(1)} %get-tuple-element.138), kind=kOutput, calls=%fused_computation.22 | convolution fusion | flops 11534336 | bytes 11714560 | tf_op jit(solution)/shard_map/sht,sthd->shd/dot_general | solution.py:89
  238.5 32.1 %all-gather.2 = f32[176,8,128]{2,1,0:T(8,128)S(1)} all-gather(f32[22,8,128]{2,1,0:T(8,128)S(1)} %bitcast.123), channel_id=4, replica_groups=mesh['kv'=8,'tp'=4] {'kv'}, dimensions={0}, use_global_device_ids=true | all-gather | bytes 811008 | tf_op jit(solution)/shard_map/all_gather | solution.py:11
  271.4 5.9 %fusion.10 = f32[22,8,1,128]{3,2,1,0:T(1,128)S(1)} fusion(bf16[22,256,8,128]{3,2,1,0:T(8,128)(2,1)} %param.22, bf16[22,8,256,1]{2,1,0,3:T(8,128)(2,1)S(1)} %get-tuple-element.136), kind=kOutput, calls=%fused_computation.20 | convolution fusion | flops 11534336 | bytes 11714560 | tf_op jit(solution)/shard_map/sht,sthd->shd/dot_general | solution.py:89
  277.3 31.7 %all-gather.5 = f32[176,8,128]{2,1,0:T(8,128)S(1)} all-gather(f32[22,8,128]{2,1,0:T(8,128)S(1)} %bitcast.124), channel_id=7, replica_groups=mesh['kv'=8,'tp'=4] {'kv'}, dimensions={0}, use_global_device_ids=true | all-gather | bytes 811008 | tf_op jit(solution)/shard_map/all_gather | solution.py:11
  310.2 10.7 %while.20 = (s32[]{:T(128)}, f32[22,8]{0,1:T(8,128)S(1)}, f32[22,8]{0,1:T(8,128)S(1)}, f32[22,8,128]{2,1,0:T(8,128)S(1)}, f32[22,8]{0,1:T(8,128)S(1)}, /*index=5...) while((s32[]{:T(128)}, f32[22,8]{0,1:T(8,128)S(1)}, ...), condition=%wide.region_8.0_spmd, body=%wide.region_7.0_spmd.sunk | while | flops 137282 | bytes 560537 | solution.py:14
  310.6 1.1 fusion.68
  312.1 1.1 fusion.68
  313.7 1.1 fusion.68
  315.2 1.1 fusion.68
  316.7 1.1 fusion.68
  318.3 1.1 fusion.68
  321.9 1.5 convolution_convert_fusion.1
  323.4 10.3 %psum.60 = bf16[22,512]{1,0:T(8,128)(2,1)S(1)} all-reduce(bf16[22,512]{1,0:T(8,128)(2,1)S(1)} %convolution_convert_fusion.1), channel_id=1, replica_groups=mesh['kv'=8,'tp'=4] {'tp'}, use_global_device_ids=true, to_apply=%region_14.15 | all-reduce | flops 11264 | bytes 45056 | tf_op jit(solution)/shard_map/psum | solution.py:132
  333.7 1.6 fusion.40
  335.2 3.4 fusion.39
  338.8 19.8 %psum.61 = f32[22,1]{0,1:T(1,128)S(1)} all-reduce(f32[22,1]{0,1:T(1,128)S(1)} %bitcast.128), channel_id=1, replica_groups=mesh['kv'=8,'tp'=4] {'kv'}, use_global_device_ids=true, to_apply=%region_16.17 | all-reduce | flops 22 | bytes 176 | tf_op jit(solution)/shard_map/psum | solution.py:137
  358.6 52.5 %all-reduce.5.cloned.1.call-done = (f32[22,2752]{1,0:T(8,128)}, f32[22,2752]{1,0:T(8,128)}) async-done(((f32[22,2752]{1,0:T(8,128)}, f32[22,2752]{1,0:T(8,128)}), (f32[22,2752]{1,0:T(8,128)}, f32[22,2752]{1,0:T(8,128)})) %all-reduce.5.cloned.1.call-update) | async-done | bytes 484368 | tf_op jit(solution)/shard_map/psum | solution.py:142
  411.1 2.5 convolution_convert_fusion
  414.4 18.8 %reduce-scatter.4.cloned.1.call-done = bf16[128,22]{1,0:T(8,128)(2,1)} async-done(((bf16[512,22]{1,0:T(8,128)(2,1)}), bf16[128,22]{1,0:T(8,128)(2,1)}) %reduce-scatter.4.cloned.1.call-update) | async-done | bytes 5648
  (112 shorter events, 11.5 us)
Async XLA Ops:
  6.5 327.1 %copy-start = (bf16[512,2752]{0,1:T(8,128)(2,1)S(1)}, bf16[512,2752]{0,1:T(8,128)(2,1)}, u32[]{:S(2)}) copy-start(bf16[512,2752]{0,1:T(8,128)(2,1)} %param.27) | copy-start | bytes 8454148
  6.5 86.7 %all-reduce.7.cloned.1.call-start = ((), (), s32[]{:S(2)}) async-start(), calls=%async_computation.3 | async-start | bytes 589824 | tf_op jit(solution)/shard_map/psum | solution.py:63
  19.5 391.6 %all-reduce.5.cloned.1.call-start = ((), (), s32[]{:S(2)}) async-start(), calls=%async_computation.2 | async-start | bytes 1081344 | tf_op jit(solution)/shard_map/psum | solution.py:142
  132.8 105.6 %copy-start.1 = (f32[8,22,8]{1,2,0:T(8,128)}, f32[8,22,8]{1,2,0:T(8,128)S(1)}, u32[]{:S(2)}) copy-start(f32[8,22,8]{1,2,0:T(8,128)S(1)} %all-gather.8) | copy-start | bytes 16900
  163.5 74.9 %copy-start.2 = (f32[8,22,8]{1,2,0:T(8,128)}, f32[8,22,8]{1,2,0:T(8,128)S(1)}, u32[]{:S(2)}) copy-start(f32[8,22,8]{1,2,0:T(8,128)S(1)} %all-gather.9) | copy-start | bytes 16900
  238.4 83.1 %copy-start.5 = (f32[8]{0:T(128)S(1)}, f32[8]{0:T(128)}, u32[]{:S(2)}) copy-start(f32[8]{0:T(128)} %param.23) | copy-start | bytes 100
  238.4 83.4 %copy-start.4 = (f32[128]{0:T(128)S(1)}, f32[128]{0:T(128)}, u32[]{:S(2)}) copy-start(f32[128]{0:T(128)} %param.24) | copy-start | bytes 1540
  238.4 71.8 %slice-start = ((f32[8,22,8]{1,2,0:T(8,128)}), f32[7,22,8]{1,2,0:T(8,128)S(1)}, s32[]{:S(2)}) async-start(f32[8,22,8]{1,2,0:T(8,128)} %copy-done.1), calls=%async_computation.4 | async-start | bytes 57344 | tf_op jit(solution)/shard_map/slice | solution.py:13
  238.4 71.8 %slice-start.1 = ((f32[8,22,8]{1,2,0:T(8,128)}), f32[7,22,8]{1,2,0:T(8,128)S(1)}, s32[]{:S(2)}) async-start(f32[8,22,8]{1,2,0:T(8,128)} %copy-done.2), calls=%async_computation.5 | async-start | bytes 57344 | tf_op jit(solution)/shard_map/slice | solution.py:13
  238.4 95.2 %copy-start.3 = (f32[512]{0:T(512)S(1)}, f32[512]{0:T(512)}, u32[]{:S(2)}) copy-start(f32[512]{0:T(512)} %param.26) | copy-start | bytes 6148
  338.6 94.6 %reduce-scatter.4.cloned.1.call-start = ((), (), s32[]{:S(2)}) async-start(), calls=%async_computation.1 | async-start | bytes 163840
Sparse Core Ops, SparseCore 0:
  19.6 73.6 all-reduce.6
  338.7 72.3 all-reduce.4
  414.5 18.6 reduce-scatter.3
where the time goes:
time: 442 us; the launch traced here: 441 us
  blocking collectives  245 us (55%)
  waiting for transfers between devices  105 us (24%)
  matrix products  41.8 us (9%)
  local copies, waits for them, and re-layouts  24.2 us (5%)
  between operations  13.3 us (3%)
  other arithmetic  11.2 us (3%)
    all_gather x6, blocking collectives, combined_all(): pieces = jax.tree.map(lambda part: lax.all_gather(part, axis), value)  186 us
    psum x1, waiting for transfers between devices, per_device(): gate_sum, up_sum = lax.psum((gate_part, up_part), 'kv')  52.5 us
    psum x1, waiting for transfers between devices, per_device(): lax.psum((query_part, key_part, value_part, jnp.sum(gathered_f * gathered...  34.2 us
    psum x1, blocking collectives, per_device(): lax.psum((query_part, key_part, value_part, jnp.sum(gathered_f * gathered...  22.2 us
    psum x1, blocking collectives, per_device(): lax.psum(jnp.sum(residual_f * residual_f, axis=1, keepdims=True), 'kv')  19.8 us
    unnamed x4, waiting for transfers between devices  18.8 us
    slice x1, local copies, waits for them, and re-layouts, partial_map(): cache_keys[:, :, :, low:high]  17.3 us
    dot_general x2, matrix products, partial_map(): jnp.einsum('shd,sthd->sht', query_rows[:, :, low:high], cache_keys[:, :,...  14.7 us
  transfers between devices with their start and end apart: 3, of which 3 were waited for; matrix products, arithmetic and copies ran while one was open for 4% of the time, Pallas kernels for 0%

commit v1 on v0

--- a/solution.py
+++ b/solution.py
@@ -134,7 +134,9 @@
     ).astype(jnp.float32)
     residual = (gathered_f + branch).astype(jnp.bfloat16)
     residual_f = residual.astype(jnp.float32)
-    mid_sum = lax.psum(jnp.sum(residual_f * residual_f, axis=1, keepdims=True), "kv")
+    mid_sum = jnp.sum(
+        lax.all_gather(jnp.sum(residual_f * residual_f, axis=1, keepdims=True), "kv"), axis=0
+    )
     scale_mid = lax.rsqrt(mid_sum / D + epsilon)
     normed_mid = (residual_f * mlp_gain).astype(jnp.bfloat16)
     gate_part = jnp.dot(normed_mid, w_gate, preferred_element_type=jnp.float32)

time: 442 us -> 442 us (level)
    psum x1 -> x0, blocking collectives: 19.8 us -> none  [per_device(): lax.psum(jnp.sum(residual_f * residual_f, axis=1, keepdims=True), 'kv')]
    unnamed x0 -> x1, blocking collectives: none -> 19.6 us
where the time goes in v1:
time: 442 us; the launch traced here: 441 us
  blocking collectives  245 us (55%)
  waiting for transfers between devices  104 us (24%)
  matrix products  41.8 us (9%)
  local copies, waits for them, and re-layouts  25.1 us (6%)
  between operations  14 us (3%)
  other arithmetic  11.2 us (3%)
    all_gather x6, blocking collectives, combined_all(): pieces = jax.tree.map(lambda part: lax.all_gather(part, axis), value)  186 us
    psum x1, waiting for transfers between devices, per_device(): gate_sum, up_sum = lax.psum((gate_part, up_part), 'kv')  50.9 us
    psum x1, waiting for transfers between devices, per_device(): lax.psum((query_part, key_part, value_part, jnp.sum(gathered_f * gathered...  34.2 us
    psum x1, blocking collectives, per_device(): lax.psum((query_part, key_part, value_part, jnp.sum(gathered_f * gathered...  22.2 us
    unnamed x1, blocking collectives  19.6 us
    unnamed x4, waiting for transfers between devices  18.8 us
    slice x1, local copies, waits for them, and re-layouts, partial_map(): cache_keys[:, :, :, low:high]  17.3 us
    dot_general x2, matrix products, partial_map(): jnp.einsum('shd,sthd->sht', query_rows[:, :, low:high], cache_keys[:, :,...  14.7 us
  transfers between devices with their start and end apart: 3, of which 3 were waited for; matrix products, arithmetic and copies ran while one was open for 4% of the time, Pallas kernels for 0%

profile of v1, /device:TPU:0, one launch (start us, length us, event | category | flops | bytes accessed | tf_op | source)
XLA Modules:
  0.0 441.0 jit_solution(8839738426164571054)
XLA Ops:
  6.5 6.5 %all_gather.42 = bf16[22,512]{1,0:T(8,128)(2,1)S(1)} all-gather(bf16[22,128]{1,0:T(8,128)(2,1)} %param.16), channel_id=1, replica_groups=mesh['kv'=8,'tp'=4] {'tp'}, dimensions={1}, use_global_device_ids=true | all-gather | bytes 28160 | tf_op jit(solution)/shard_map/all_gather | solution.py:57
  13.0 2.1 fusion.35
  15.2 2.1 fusion.33
  17.3 2.1 fusion.37
  19.5 17.3 %fusion.54 = (bf16[22,256,8,64]{3,2,1,0:T(8,128)(2,1)}, bf16[22,256,8,64]{3,2,1,0:T(8,128)(2,1)}) fusion(bf16[22,256,8,128]{3,2,1,0:T(8,128)(2,1)} %param.21), kind=kLoop, calls=%fused_computation.89 | loop fusion | bytes 23068672 | tf_op jit(solution)/shard_map/slice | solution.py:81
  36.9 22.2 %psum.49 = f32[22,1]{0,1:T(1,128)S(1)} all-reduce(f32[22,1]{0,1:T(1,128)S(1)} %bitcast.126), channel_id=1, replica_groups=mesh['kv'=8,'tp'=4] {'kv'}, use_global_device_ids=true, to_apply=%region_1.0 | all-reduce | flops 22 | bytes 176 | tf_op jit(solution)/shard_map/psum | solution.py:63
  59.1 34.2 %all-reduce.8.cloned.1.call-done = (f32[22,1024]{1,0:T(8,128)}, f32[22,1024]{1,0:T(8,128)}, f32[22,1024]{1,0:T(8,128)}) async-done(((f32[22,1024]{1,0:T(8,128)}, f32[22,1024]{1,0:T(8,128)}, f32[22,1024]{1,0:T(8,128)}), (f32[22,1024]{1,0:T(8,128)}, f32[22,1024]{1,0:T(8,128)}, f32[22,1024]{1,0:T(8,128)})) %all-reduce.8.cloned.1.call-update) | async-done | bytes 270352 | tf_op jit(solution)/shard_map/psum | solution.py:63
  94.5 7.4 %fusion.6 = f32[22,8,1,256]{3,2,1,0:T(1,128)S(1)} fusion(bf16[22,256,8,64]{3,2,1,0:T(8,128)(2,1)} %get-tuple-element.134, bf16[22,8,64,1]{2,1,0,3:T(8,128)(2,1)S(1)} %get-tuple-element.142), kind=kOutput, calls=%fused_computation.16 | convolution fusion | flops 5767168 | bytes 5969920 | tf_op jit(solution)/shard_map/shd,sthd->sht/dot_general | solution.py:78
  102.2 30.6 %all-gather.9 = f32[8,22,8]{1,2,0:T(8,128)S(1)} all-gather(f32[1,22,8]{1,2,0:T(8,128)S(1)} %copy.59), channel_id=5, replica_groups=mesh['kv'=8,'tp'=4] {'kv'}, dimensions={0}, use_global_device_ids=true | all-gather | bytes 6336 | tf_op jit(solution)/shard_map/all_gather | solution.py:11
  132.9 30.6 %all-gather.10 = f32[8,22,8]{1,2,0:T(8,128)S(1)} all-gather(f32[1,22,8]{1,2,0:T(8,128)S(1)} %copy.60), channel_id=6, replica_groups=mesh['kv'=8,'tp'=4] {'kv'}, dimensions={0}, use_global_device_ids=true | all-gather | bytes 6336 | tf_op jit(solution)/shard_map/all_gather | solution.py:11
  163.5 7.4 %fusion.8 = f32[22,8,1,256]{3,2,1,0:T(1,128)S(1)} fusion(bf16[22,256,8,64]{3,2,1,0:T(8,128)(2,1)} %get-tuple-element.135, bf16[22,8,64,1]{2,1,0,3:T(8,128)(2,1)S(1)} %get-tuple-element.143), kind=kOutput, calls=%fused_computation.18 | convolution fusion | flops 5767168 | bytes 5969920 | tf_op jit(solution)/shard_map/shd,sthd->sht/dot_general | solution.py:78
  171.2 30.6 %all-gather.7 = f32[8,22,8]{1,2,0:T(8,128)S(1)} all-gather(f32[1,22,8]{1,2,0:T(8,128)S(1)} %copy.57), channel_id=2, replica_groups=mesh['kv'=8,'tp'=4] {'kv'}, dimensions={0}, use_global_device_ids=true | all-gather | bytes 6336 | tf_op jit(solution)/shard_map/all_gather | solution.py:11
  201.9 30.6 %all-gather.8 = f32[8,22,8]{1,2,0:T(8,128)S(1)} all-gather(f32[1,22,8]{1,2,0:T(8,128)S(1)} %copy.58), channel_id=3, replica_groups=mesh['kv'=8,'tp'=4] {'kv'}, dimensions={0}, use_global_device_ids=true | all-gather | bytes 6336 | tf_op jit(solution)/shard_map/all_gather | solution.py:11
  232.5 5.9 %fusion.12 = f32[22,8,1,128]{3,2,1,0:T(1,128)S(1)} fusion(bf16[22,256,8,128]{3,2,1,0:T(8,128)(2,1)} %param.22, bf16[22,8,256,1]{2,1,0,3:T(8,128)(2,1)S(1)} %get-tuple-element.138), kind=kOutput, calls=%fused_computation.22 | convolution fusion | flops 11534336 | bytes 11714560 | tf_op jit(solution)/shard_map/sht,sthd->shd/dot_general | solution.py:89
  238.5 32.1 %all-gather.2 = f32[176,8,128]{2,1,0:T(8,128)S(1)} all-gather(f32[22,8,128]{2,1,0:T(8,128)S(1)} %bitcast.121), channel_id=4, replica_groups=mesh['kv'=8,'tp'=4] {'kv'}, dimensions={0}, use_global_device_ids=true | all-gather | bytes 811008 | tf_op jit(solution)/shard_map/all_gather | solution.py:11
  271.4 5.9 %fusion.10 = f32[22,8,1,128]{3,2,1,0:T(1,128)S(1)} fusion(bf16[22,256,8,128]{3,2,1,0:T(8,128)(2,1)} %param.22, bf16[22,8,256,1]{2,1,0,3:T(8,128)(2,1)S(1)} %get-tuple-element.136), kind=kOutput, calls=%fused_computation.20 | convolution fusion | flops 11534336 | bytes 11714560 | tf_op jit(solution)/shard_map/sht,sthd->shd/dot_general | solution.py:89
  277.3 31.7 %all-gather.5 = f32[176,8,128]{2,1,0:T(8,128)S(1)} all-gather(f32[22,8,128]{2,1,0:T(8,128)S(1)} %bitcast.122), channel_id=7, replica_groups=mesh['kv'=8,'tp'=4] {'kv'}, dimensions={0}, use_global_device_ids=true | all-gather | bytes 811008 | tf_op jit(solution)/shard_map/all_gather | solution.py:11
  310.3 10.7 %while.20 = (s32[]{:T(128)}, f32[22,8]{0,1:T(8,128)S(1)}, f32[22,8]{0,1:T(8,128)S(1)}, f32[22,8,128]{2,1,0:T(8,128)S(1)}, f32[22,8]{0,1:T(8,128)S(1)}, /*index=5...) while((s32[]{:T(128)}, f32[22,8]{0,1:T(8,128)S(1)}, ...), condition=%wide.region_8.0_spmd, body=%wide.region_7.0_spmd.sunk | while | flops 137282 | bytes 560537 | solution.py:14
  310.6 1.1 fusion.68
  312.2 1.1 fusion.68
  313.7 1.1 fusion.68
  315.2 1.1 fusion.68
  316.7 1.1 fusion.68
  318.3 1.1 fusion.68
  321.9 1.5 convolution_convert_fusion.1
  323.4 10.3 %psum.53 = bf16[22,512]{1,0:T(8,128)(2,1)S(1)} all-reduce(bf16[22,512]{1,0:T(8,128)(2,1)S(1)} %convolution_convert_fusion.1), channel_id=1, replica_groups=mesh['kv'=8,'tp'=4] {'tp'}, use_global_device_ids=true, to_apply=%region_14.15 | all-reduce | flops 11264 | bytes 45056 | tf_op jit(solution)/shard_map/psum | solution.py:132
  333.7 1.6 fusion.40
  335.2 3.4 fusion.39
  340.3 19.6 %all-reduce = f32[176]{0:T(256)S(1)} all-reduce(f32[176]{0:T(256)S(1)} %dynamic-update-slice), channel_id=8, replica_groups=mesh['kv'=8,'tp'=4] {'kv'}, use_global_device_ids=true, to_apply=%add | all-reduce | flops 176 | bytes 1408
  360.0 50.9 %all-reduce.6.cloned.1.call-done = (f32[22,2752]{1,0:T(8,128)}, f32[22,2752]{1,0:T(8,128)}) async-done(((f32[22,2752]{1,0:T(8,128)}, f32[22,2752]{1,0:T(8,128)}), (f32[22,2752]{1,0:T(8,128)}, f32[22,2752]{1,0:T(8,128)})) %all-reduce.6.cloned.1.call-update) | async-done | bytes 484368 | tf_op jit(solution)/shard_map/psum | solution.py:144
  410.9 2.5 convolution_convert_fusion
  414.2 18.8 %reduce-scatter.4.cloned.1.call-done = bf16[128,22]{1,0:T(8,128)(2,1)} async-done(((bf16[512,22]{1,0:T(8,128)(2,1)}), bf16[128,22]{1,0:T(8,128)(2,1)}) %reduce-scatter.4.cloned.1.call-update) | async-done | bytes 5648
  (119 shorter events, 12.4 us)
Async XLA Ops:
  6.5 327.1 %copy-start = (bf16[512,2752]{0,1:T(8,128)(2,1)S(1)}, bf16[512,2752]{0,1:T(8,128)(2,1)}, u32[]{:S(2)}) copy-start(bf16[512,2752]{0,1:T(8,128)(2,1)} %param.27) | copy-start | bytes 8454148
  6.5 86.7 %all-reduce.8.cloned.1.call-start = ((), (), s32[]{:S(2)}) async-start(), calls=%async_computation.3 | async-start | bytes 589824 | tf_op jit(solution)/shard_map/psum | solution.py:63
  19.5 391.4 %all-reduce.6.cloned.1.call-start = ((), (), s32[]{:S(2)}) async-start(), calls=%async_computation.2 | async-start | bytes 1081344 | tf_op jit(solution)/shard_map/psum | solution.py:144
  132.8 105.6 %copy-start.1 = (f32[8,22,8]{1,2,0:T(8,128)}, f32[8,22,8]{1,2,0:T(8,128)S(1)}, u32[]{:S(2)}) copy-start(f32[8,22,8]{1,2,0:T(8,128)S(1)} %all-gather.9) | copy-start | bytes 16900
  163.5 74.9 %copy-start.2 = (f32[8,22,8]{1,2,0:T(8,128)}, f32[8,22,8]{1,2,0:T(8,128)S(1)}, u32[]{:S(2)}) copy-start(f32[8,22,8]{1,2,0:T(8,128)S(1)} %all-gather.10) | copy-start | bytes 16900
  238.4 83.1 %copy-start.5 = (f32[8]{0:T(128)S(1)}, f32[8]{0:T(128)}, u32[]{:S(2)}) copy-start(f32[8]{0:T(128)} %param.23) | copy-start | bytes 100
  238.4 83.4 %copy-start.4 = (f32[128]{0:T(128)S(1)}, f32[128]{0:T(128)}, u32[]{:S(2)}) copy-start(f32[128]{0:T(128)} %param.24) | copy-start | bytes 1540
  238.4 71.8 %slice-start = ((f32[8,22,8]{1,2,0:T(8,128)}), f32[7,22,8]{1,2,0:T(8,128)S(1)}, s32[]{:S(2)}) async-start(f32[8,22,8]{1,2,0:T(8,128)} %copy-done.1), calls=%async_computation.4 | async-start | bytes 57344 | tf_op jit(solution)/shard_map/slice | solution.py:13
  238.4 71.8 %slice-start.1 = ((f32[8,22,8]{1,2,0:T(8,128)}), f32[7,22,8]{1,2,0:T(8,128)S(1)}, s32[]{:S(2)}) async-start(f32[8,22,8]{1,2,0:T(8,128)} %copy-done.2), calls=%async_computation.5 | async-start | bytes 57344 | tf_op jit(solution)/shard_map/slice | solution.py:13
  238.4 95.2 %copy-start.3 = (f32[512]{0:T(512)S(1)}, f32[512]{0:T(512)}, u32[]{:S(2)}) copy-start(f32[512]{0:T(512)} %param.26) | copy-start | bytes 6148
  271.4 67.3 %copy-start.6 = (u32[32]{0:T(128)S(1)}, u32[32]{0:T(128)}, u32[]{:S(2)}) copy-start(u32[32]{0:T(128)} %constant.45) | copy-start | bytes 388
  338.6 94.4 %reduce-scatter.4.cloned.1.call-start = ((), (), s32[]{:S(2)}) async-start(), calls=%async_computation.1 | async-start | bytes 163840
Sparse Core Ops, SparseCore 0:
  19.6 73.6 all-reduce.7
  338.7 72.1 all-reduce.5
  414.3 18.6 reduce-scatter.3
